TPU v7x, 32 devices: a whole 2x2x4 slice. The times are simulated.
32 devices in a mesh: rep: 2 (over y), fs: 4 (over z), tp: 4 (over x, core).
Axes of the slice: x: 2, y: 2, z: 4, core: 2. Of those that a mesh axis runs over, the one named last changes fastest.
Arguments:
- activations: bfloat16 [3072, 2048], P(('rep', 'fs'), 'tp'), may hold values from -16 to 16
- norm_gain: float32 [2048], replicated, may hold values from 0.1 to 1.9
- query_weight: bfloat16 [2048, 512], P('fs', 'tp'), may hold values from -0.125 to 0.125
- key_weight: bfloat16 [2048, 512], P('fs', 'tp'), may hold values from -0.125 to 0.125
- value_weight: bfloat16 [2048, 512], P('fs', 'tp'), may hold values from -0.125 to 0.125
- gate_weight: bfloat16 [2048, 512], P('fs', 'tp'), may hold values from -0.125 to 0.125
- out_weight: bfloat16 [512, 2048], P('tp', 'fs'), may hold values from -0.25 to 0.25
- mlp_gain: float32 [2048], replicated, may hold values from 0.1 to 1.9
- up_weight: bfloat16 [2048, 8192], P('fs', 'tp'), may hold values from -0.125 to 0.125
- down_weight: bfloat16 [8192, 2048], P('tp', 'fs'), may hold values from -0.0625 to 0.0625
Outputs:
- layer_out: bfloat16 [3072, 2048], P(('rep', 'fs'), 'tp')
All inputs are finite; a program needn't handle non-finite values.
Results may differ from a plain program's by a relative error of at most 0.012.
Values may be sent and summed in bfloat16 or wider, within the bound.
A program may use at most 64 MiB of HBM per device.

v0:
```python
import functools

import jax
import jax.numpy as jnp
import numpy as np
from jax import lax
from jax.experimental import pallas as pl
from jax.experimental.pallas import tpu as pltpu
from jax.sharding import PartitionSpec as P

HEADS = 8
HEAD_DIM = 64
SEQ_LEN = 128
EPSILON = 1e-06
MESH = pl.DeviceIdType.MESH
BF16 = jnp.bfloat16
F32 = jnp.float32


def tables(head_width):
    half = HEAD_DIM // 2
    freqs = np.float32(10000.0) ** (-np.arange(half, dtype=np.float32) / np.float32(half))
    angle = np.arange(SEQ_LEN, dtype=np.float32)[:, None] * freqs[None, :]
    lane = np.arange(2 * head_width)
    scale = np.where(lane < head_width, 1.0, HEAD_DIM**-0.5).astype(np.float32)
    sign = np.where(lane % HEAD_DIM < half, -1.0, 1.0).astype(np.float32)
    cosine = np.cos(angle)[:, lane % half] * scale
    sine = np.sin(angle)[:, lane % half] * scale * sign
    exponent = np.float32(5.0) + np.float32(4.0) * np.arange(HEADS, dtype=np.float32) / np.float32(HEADS - 1)
    log_gamma = np.log(np.float32(1.0) - np.power(np.float32(2.0), -exponent))
    place = np.arange(SEQ_LEN, dtype=np.float32)
    distance = place[:, None] - place[None, :]
    decay = np.where(
        distance[None] >= 0,
        np.exp(np.maximum(distance, 0.0)[None] * log_gamma[:, None, None]),
        0.0,
    )
    return cosine.astype(np.float32), sine.astype(np.float32), decay.astype(np.float32)


class Plan:
    def __init__(self):
        self.size = 0

    def take(self, count):
        base = self.size
        self.size += count
        return base


def build(mesh_shape, shapes):
    R, F, T = mesh_shape["rep"], mesh_shape["fs"], mesh_shape["tp"]
    X, HF, Q = T // 2, F // 2, F // T
    n, dc = shapes["activations"]
    dep, hw = shapes["query_weight"]
    fw = shapes["up_weight"][1]
    D = dc * T
    hid = fw // 2
    seqs = n // SEQ_LEN
    local_heads = hw // HEAD_DIM
    n_small = 4 if hw % 128 == 0 else 1
    sw = 4 * hw // n_small

    plan = Plan()
    L_ACT, L_OUT, L_UP, L_DOWN, L_DECAY, L_SMALL = (
        plan.take(1),
        plan.take(1),
        plan.take(1),
        plan.take(1),
        plan.take(1),
        plan.take(n_small),
    )

    class Spread:
        def __init__(self):
            self.send, self.recv = plan.take(2 * X - 1), plan.take(T)

    act_spread = Spread()
    ret_spread = [Spread() for _ in range(seqs)]
    mid_spread = [Spread() for _ in range(2)]
    mid_z = (plan.take(1), plan.take(1))
    om_send, om_recv = plan.take((T - 1) * Q), plan.take(T * Q)

    class Stream:
        def __init__(self):
            self.zs, self.zf, self.zr = plan.take(max(F, 3)), plan.take(F), plan.take(F)
            self.ys, self.yr = plan.take(F * R), plan.take(F * R)

    qkv_stream, out_stream, up_stream, down_stream = Stream(), Stream(), Stream(), Stream()
    ps, pr = plan.take(2 * F), plan.take(2 * F)
    xs, xr = plan.take(2 * F), plan.take(2 * max(X - 1, 1) * Q)
    fz_s, fz_r = plan.take(Q), plan.take(Q)

    def kernel(*refs):
        act = refs[0]
        small = refs[1 : 1 + n_small]
        (out_w, up_w, down_w, gain1, gain2, cosine, sine, decay_all, result) = refs[1 + n_small : 10 + n_small]
        (
            act_full,
            normed,
            wbuf,
            proj,
            decay,
            og,
            om,
            ret,
            mid,
            second,
            upb,
            dnb,
            acc,
            hidden,
            pf,
            pbuf,
            srecv,
            tot,
            xrecv,
            zsnd,
            zrecv,
            sem,
        ) = refs[10 + n_small :]
        r, f, t = lax.axis_index("rep"), lax.axis_index("fs"), lax.axis_index("tp")
        x, c = t // 2, t % 2
        sib = 2 * x + 1 - c
        h = f // HF
        partner = (f + HF) % F

        def order(k):
            g = h * (F - 1 - f) + (1 - h) * f
            past = (k + 2 * F - 2 * g - 1) // (2 * F)
            odd = k % 2
            near = g + odd * ((k + 1) // 2) - (1 - odd) * (k // 2)
            s = past * k + (1 - past) * near
            return h * (F - 1 - s) + (1 - h) * s

        def at(i):
            return sem.at[i]

        def remote(src, dst, send, recv, **where):
            return pltpu.make_async_remote_copy(
                src_ref=src,
                dst_ref=dst,
                send_sem=at(send),
                recv_sem=at(recv),
                device_id=where,
                device_id_type=MESH,
            )

        def local(src, dst, i):
            return pltpu.make_async_copy(src, dst, at(i))

        def span(start, size, unit):
            return pl.ds(pl.multiple_of(start, unit), size)

        def act_block(s):
            return act_full.at[:, span(s * dc, dc, dc)]

        def mid_block(g, s):
            return mid.at[g, :, span(s * dc, dc, dc)]

        def ret_block(j, s):
            return ret.at[s, pl.ds(j * SEQ_LEN, SEQ_LEN), :]

        def qkv_part(s, part):
            rows = dep // R
            return wbuf.at[span(s * dep + part * rows, rows, rows), :]

        def out_part(s, part):
            rows = hw // R
            return og.at[s, span(part * rows, rows, rows), :]

        def up_part(s, part):
            rows = dep // R
            return upb.at[span(s * dep + part * rows, rows, rows), :]

        def down_part(s, part):
            rows = hid // R
            return dnb.at[s, span(part * rows, rows, rows), :]

        def up_own(half):
            rows = dep // R
            return up_w.at[span(r * rows, rows, rows), span(half * hid, hid, hid)]

        def down_own(half):
            rows = hid // R
            return down_w.at[span(half * hid + r * rows, rows, rows), :]

        def spread_copies(sp, block, source):
            first = [remote(source, block(t), sp.send, sp.recv + t, tp=sib)]
            for j in range(1, X):
                first.append(remote(source, block(t), sp.send + j, sp.recv + t, tp=((x + j) % X) * 2 + c))
            return first

        def spread_start(sp, block, source):
            for copy in reversed(spread_copies(sp, block, source)):
                copy.start()

        def relay_copy(sp, block, j):
            s = ((x + X - j) % X) * 2 + c
            return remote(block(s), block(s), sp.send + X - 1 + j, sp.recv + s, tp=sib)

        def spread_relay(sp, block):
            for j in range(1, X):
                s = ((x + X - j) % X) * 2 + c
                remote(block(s), block(s), sp.send, sp.recv + s, tp=sib).wait_recv()
                relay_copy(sp, block, j).start()

        def spread_finish(sp, block):
            for j in range(X):
                s = ((x + X - j) % X) * 2 + 1 - c
                remote(block(s), block(s), sp.send, sp.recv + s, tp=sib).wait_recv()

        def spread_drain(sp, block, source):
            for copy in spread_copies(sp, block, source):
                copy.wait_send()
            for j in range(1, X):
                relay_copy(sp, block, j).wait_send()

        def y_copy(st, part, s, q):
            return remote(
                part(s, r), part(s, r), st.ys + s * R + q, st.yr + s * R + r, rep=(r + q) % R
            )

        def y_start(st, part, s):
            for q in range(1, R):
                y_copy(st, part, s, q).start()

        def y_wait(st, part, s):
            for q in range(1, R):
                other = (r + R - q) % R
                remote(
                    part(s, other), part(s, other), st.ys, st.yr + s * R + other, rep=other
                ).wait_recv()

        def z_wait(st, part, s):
            remote(part(s, r), part(s, r), st.zs, st.zr + s, fs=s).wait_recv()

        def direct_copy(st, part, k):
            return remote(part(f, r), part(f, r), st.zs + k, st.zr + f, fs=order(k))

        def own_copies(st, part, own):
            return (
                remote(own(1 - h), part(f, r), st.zs, st.zr + f, fs=HF - h),
                remote(own(h), part(f, r), st.zs + 1, st.zr + f, fs=(f + 1) % F),
                remote(own(h), part(f, r), st.zs + 2, st.zr + f, fs=(f + F - 1) % F),
            )

        def own_do(st, part, own, what):
            across, onward, back = own_copies(st, part, own)
            what(across)

            @pl.when(f % HF != HF - 1)
            def _():
                what(onward)

            @pl.when(f % HF != 0)
            def _():
                what(back)

        def forward_do(st, part, s, what):
            after = f + 2 * ((f - s + F) // F) - 1

            @pl.when((after + HF) // HF - 1 == h)
            def _():
                what(remote(part(s, r), part(s, r), st.zf + s, st.zr + s, fs=(after + F) % F))

        def pass_on(st, part, k):
            s = order(k)
            z_wait(st, part, s)
            forward_do(st, part, s, lambda copy: copy.start())
            y_start(st, part, s)

        head0 = t * local_heads
        loads = [local(act, act_block(t), L_ACT)]
        for i in range(n_small):
            loads.append(local(small[i], wbuf.at[span(f * dep, dep, dep), pl.ds(i * sw, sw)], L_SMALL + i))
        loads.append(local(out_w, og.at[f], L_OUT))
        loads.append(local(decay_all.at[pl.ds(head0, local_heads)], decay, L_DECAY))
        loads.append(local(up_w.at[:, span(h * hid, hid, hid)], upb.at[span(f * dep, dep, dep), :], L_UP))
        loads.append(local(down_w.at[span(h * hid, hid, hid), :], dnb.at[f], L_DOWN))
        for copy in loads:
            copy.start()

        barrier = pltpu.get_barrier_semaphore()
        for j in range(1, T):
            pl.semaphore_signal(barrier, inc=1, device_id={"tp": (t + j) % T}, device_id_type=MESH)
        for j in range(1, F):
            pl.semaphore_signal(barrier, inc=1, device_id={"fs": (f + j) % F}, device_id_type=MESH)
        for j in range(1, R):
            pl.semaphore_signal(barrier, inc=1, device_id={"rep": (r + j) % R}, device_id_type=MESH)
        pl.semaphore_wait(barrier, T + F + R - 3)

        spread_start(act_spread, act_block, act)
        for i in range(n_small):
            loads[1 + i].wait()
        for k in range(1, F):
            direct_copy(qkv_stream, qkv_part, k).start()
        loads[1 + n_small].wait()
        for k in range(1, F):
            direct_copy(out_stream, out_part, k).start()
        own_do(up_stream, up_part, up_own, lambda copy: copy.start())
        loads[0].wait()
        for copy in loads[2 + n_small :]:
            copy.wait()

        spread_relay(act_spread, act_block)
        spread_finish(act_spread, act_block)
        step = 64

        def norm_rows(source, gain, target):
            rows = source.astype(F32)
            mean = jnp.mean(rows * rows, axis=-1, keepdims=True)
            target[...] = (rows * lax.rsqrt(mean + EPSILON) * gain[...]).astype(BF16)

        def norm_first(i, carry):
            rows = span(i * step, step, step)
            norm_rows(act_full[rows, :], gain1, normed.at[rows, :])
            return carry

        lax.fori_loop(0, n // step, norm_first, 0)

        def project(k):
            s = order(k)
            part = jnp.dot(
                normed[:, span(s * dep, dep, dep)],
                wbuf[span(s * dep, dep, dep), :],
                preferred_element_type=F32,
            )
            if isinstance(k, int):
                proj[...] = part
            else:
                proj[...] += part

        project(0)

        def small_on(k, carry):
            s = order(k)
            z_wait(qkv_stream, qkv_part, s)
            y_start(qkv_stream, qkv_part, s)
            return carry

        lax.fori_loop(1, F, small_on, 0)

        def out_on(k, carry):
            s = order(k)
            z_wait(out_stream, out_part, s)
            y_start(out_stream, out_part, s)
            return carry

        lax.fori_loop(1, F, out_on, 0)

        def small_use(k, carry):
            y_wait(qkv_stream, qkv_part, order(k))
            project(k)
            return carry

        lax.fori_loop(1, F, small_use, 0)

        def out_take(k, carry):
            y_wait(out_stream, out_part, order(k))
            return carry

        lax.fori_loop(1, F, out_take, 0)

        def om_copy(j, i):
            to = (t + j) % T
            return remote(
                og.at[to * Q + i],
                om.at[i, span(t * hw, hw, hw), :],
                om_send + (j - 1) * Q + i,
                om_recv + t * Q + i,
                tp=to,
            )

        for j in range(1, T):
            for i in range(Q):
                om_copy(j, i).start()
        for i in range(Q):
            om[i, span(t * hw, hw, hw), :] = og[t * Q + i]

        lane = lax.broadcasted_iota(jnp.int32, (SEQ_LEN, 2 * hw), 1)
        first_half = lane % HEAD_DIM < HEAD_DIM // 2
        head_of = lax.broadcasted_iota(jnp.int32, (SEQ_LEN, hw), 1) // HEAD_DIM

        def of_head(values, i):
            return values if local_heads == 1 else jnp.where(head_of == i, values, 0.0)

        def head_mean(values):
            total = jnp.zeros_like(values)
            for i in range(local_heads):
                mean = jnp.sum(of_head(values, i), axis=-1, keepdims=True) * (1.0 / HEAD_DIM)
                total += of_head(jnp.broadcast_to(mean, values.shape), i)
            return total

        for j in range(seqs):
            rows = pl.ds(j * SEQ_LEN, SEQ_LEN)
            raw = proj[rows, : 2 * hw]
            turned = jnp.where(
                first_half,
                pltpu.roll(raw, 2 * hw - HEAD_DIM // 2, 1),
                pltpu.roll(raw, HEAD_DIM // 2, 1),
            )
            both = raw * cosine[...] + turned * sine[...]
            query, key = both[:, :hw], both[:, hw:].astype(BF16)
            value = proj[rows, 2 * hw : 3 * hw]
            gate = proj[rows, 3 * hw :]
            mixed = jnp.zeros((SEQ_LEN, hw), F32)
            for i in range(local_heads):
                scores = lax.dot_general(
                    of_head(query, i).astype(BF16), key, (((1,), (1,)), ((), ())), preferred_element_type=F32
                )
                weights = (scores * decay[i]).astype(BF16)
                mixed += jnp.dot(weights, of_head(value, i).astype(BF16), preferred_element_type=F32)
            centred = mixed - head_mean(mixed)
            spread_of = lax.rsqrt(head_mean(centred * centred) + EPSILON)
            ret[t, rows, :] = (centred * spread_of * (gate * jax.nn.sigmoid(gate))).astype(BF16)
            block = functools.partial(ret_block, j)
            spread_start(ret_spread[j], block, block(t))

        pass_on(up_stream, up_part, 1)

        for j in range(1, T):
            s = (t + T - j) % T
            for i in range(Q):
                block = om.at[i, span(s * hw, hw, hw), :]
                remote(block, block, om_send, om_recv + s * Q + i, tp=s).wait_recv()
        for j in range(seqs):
            spread_relay(ret_spread[j], functools.partial(ret_block, j))
        for j in range(seqs):
            block = functools.partial(ret_block, j)
            spread_finish(ret_spread[j], block)
            rows = pl.ds(j * SEQ_LEN, SEQ_LEN)
            for i in range(Q):
                branch = jnp.zeros((SEQ_LEN, dep), F32)
                for s in range(T):
                    branch += jnp.dot(
                        ret[s, rows, :], om[i, pl.ds(s * hw, hw), :], preferred_element_type=F32
                    )
                columns = span(t * dc + i * dep, dep, dep)
                mid[0, rows, columns] = (act_full[rows, columns].astype(F32) + branch).astype(BF16)
        mid_own = functools.partial(mid_block, 0)
        mid_other = functools.partial(mid_block, 1)
        spread_start(mid_spread[0], mid_own, mid_own(t))
        to_partner = remote(mid_own(t), mid_other(t), mid_z[0], mid_z[1], fs=partner)
        to_partner.start()
        own_do(down_stream, down_part, down_own, lambda copy: copy.start())

        def up_on(k, carry):
            pass_on(up_stream, up_part, k)
            return carry

        lax.fori_loop(2, F, up_on, 0)

        spread_relay(mid_spread[0], mid_own)
        spread_finish(mid_spread[0], mid_own)

        def norm_second(g):
            def body(i, carry):
                rows = span(i * step, step, step)
                norm_rows(mid[g, rows, :], gain2, second.at[g, rows, :])
                return carry

            lax.fori_loop(0, n // step, body, 0)

        norm_second(0)
        to_partner.wait_recv()
        spread_start(mid_spread[1], mid_other, mid_other(t))
        spread_relay(mid_spread[1], mid_other)
        spread_finish(mid_spread[1], mid_other)
        norm_second(1)

        def raise_by(k):
            s = order(k)
            for g in range(2):
                part = jnp.dot(
                    second[g, :, span(s * dep, dep, dep)],
                    upb[span(s * dep, dep, dep), :],
                    preferred_element_type=F32,
                )
                if isinstance(k, int):
                    acc[g] = part
                else:
                    acc[g] += part

        raise_by(0)

        def up_use(k, carry):
            y_wait(up_stream, up_part, order(k))
            raise_by(k)
            return carry

        lax.fori_loop(1, F, up_use, 0)
        for g in range(2):
            kept = jnp.maximum(acc[g], 0.0)
            hidden[g] = (kept * kept).astype(BF16)

        def where_to(k):
            s = order(k)
            return s, s // Q, s % Q

        def lower(k):
            s, td, i = where_to(k)
            xd, cd = td // 2, td % 2
            for g in (1, 0):
                pf[g] = jnp.dot(hidden[g], dnb[s], preferred_element_type=F32)

                @pl.when(c != cd)
                def _():
                    pbuf[s, g] = pf[g].astype(BF16)
                    remote(
                        pbuf.at[s, g], srecv.at[s, g], ps + 2 * s + g, pr + 2 * s + g, tp=sib
                    ).start()

            @pl.when(c == cd)
            def _():
                for g in (1, 0):
                    remote(
                        pbuf.at[s, g], srecv.at[s, g], ps + 2 * s + g, pr + 2 * s + g, tp=sib
                    ).wait_recv()
                    total = pf[g] + srecv[s, g].astype(F32)

                    @pl.when(x == xd)
                    def _():
                        tot[g, i] = total

                    @pl.when(x != xd)
                    def _():
                        pbuf[s, g] = total.astype(BF16)
                        x_copy(s, g).start()

        def x_copy(s, g):
            td, i = s // Q, s % Q
            away = (x + X - td // 2) % X
            slot = (away + X - 1) % X % max(X - 1, 1)
            return remote(
                pbuf.at[s, g],
                xrecv.at[slot, g, i],
                xs + 2 * s + g,
                xr + (slot * 2 + g) * Q + i,
                tp=(td // 2) * 2 + c,
            )

        def z_copy(i):
            return remote(zsnd.at[i], zrecv.at[i], fz_s + i, fz_r + i, fs=partner)

        def settle(k):
            s, td, i = where_to(k)

            @pl.when(td == t)
            def _():
                for g in (1, 0):
                    total = tot[g, i]
                    for slot in range(X - 1):
                        block = xrecv.at[slot, g, i]
                        remote(block, block, xs, xr + (slot * 2 + g) * Q + i, tp=sib).wait_recv()
                        total += xrecv[slot, g, i].astype(F32)
                    if g == 1:
                        zsnd[i] = total.astype(BF16)
                        z_copy(i).start()
                    else:
                        tot[0, i] = total

        lower(0)

        def down_use(k, carry):
            pass_on(down_stream, down_part, k)
            y_wait(down_stream, down_part, order(k))
            lower(k)
            settle(k - 1)
            return carry

        lax.fori_loop(1, F, down_use, 0)
        settle(F - 1)
        for i in range(Q):
            z_copy(i).wait_recv()
            columns = span(t * dc + i * dep, dep, dep)
            result[:, i * dep : (i + 1) * dep] = (
                mid[0, :, columns].astype(F32) + (tot[0, i] + zrecv[i].astype(F32))
            ).astype(BF16)

        spread_drain(act_spread, act_block, act)
        for j in range(seqs):
            block = functools.partial(ret_block, j)
            spread_drain(ret_spread[j], block, block(t))
        spread_drain(mid_spread[0], mid_own, mid_own(t))
        spread_drain(mid_spread[1], mid_other, mid_other(t))
        to_partner.wait_send()
        for j in range(1, T):
            for i in range(Q):
                om_copy(j, i).wait_send()
        for i in range(Q):
            z_copy(i).wait_send()
        own_do(up_stream, up_part, up_own, lambda copy: copy.wait_send())
        own_do(down_stream, down_part, down_own, lambda copy: copy.wait_send())

        def sent(k, carry):
            s = order(k)
            direct_copy(qkv_stream, qkv_part, k).wait_send()
            direct_copy(out_stream, out_part, k).wait_send()
            forward_do(up_stream, up_part, s, lambda copy: copy.wait_send())
            forward_do(down_stream, down_part, s, lambda copy: copy.wait_send())
            for st, part in (
                (qkv_stream, qkv_part),
                (out_stream, out_part),
                (up_stream, up_part),
                (down_stream, down_part),
            ):
                for q in range(1, R):
                    y_copy(st, part, s, q).wait_send()
            return carry

        lax.fori_loop(1, F, sent, 0)

        def summed(k, carry):
            s, td, i = where_to(k)
            for g in range(2):

                @pl.when(c != td % 2)
                def _():
                    remote(
                        pbuf.at[s, g], srecv.at[s, g], ps + 2 * s + g, pr + 2 * s + g, tp=sib
                    ).wait_send()

                @pl.when((c == td % 2) & (x != td // 2))
                def _():
                    x_copy(s, g).wait_send()

            return carry

        lax.fori_loop(0, F, summed, 0)

    vmem = pltpu.VMEM
    scratch = [
        vmem((n, D), BF16),
        vmem((n, D), BF16),
        vmem((D, 4 * hw), BF16),
        vmem((n, 4 * hw), F32),
        vmem((local_heads, SEQ_LEN, SEQ_LEN), F32),
        vmem((F, hw, dep), BF16),
        vmem((Q, T * hw, dep), BF16),
        vmem((T, n, hw), BF16),
        vmem((2, n, D), BF16),
        vmem((2, n, D), BF16),
        vmem((D, hid), BF16),
        vmem((F, hid, dep), BF16),
        vmem((2, n, hid), F32),
        vmem((2, n, hid), BF16),
        vmem((2, n, dep), F32),
        vmem((F, 2, n, dep), BF16),
        vmem((F, 2, n, dep), BF16),
        vmem((2, Q, n, dep), F32),
        vmem((max(X - 1, 1), 2, Q, n, dep), BF16),
        vmem((Q, n, dep), BF16),
        vmem((Q, n, dep), BF16),
        pltpu.SemaphoreType.DMA((plan.size,)),
    ]
    anywhere = pl.BlockSpec(memory_space=pl.ANY)
    in_vmem = pl.BlockSpec(memory_space=vmem)
    call = pl.pallas_call(
        kernel,
        name="layer",
        out_shape=jax.ShapeDtypeStruct((n, dc), BF16),
        in_specs=[anywhere] * (1 + n_small + 3) + [in_vmem] * 4 + [anywhere],
        out_specs=in_vmem,
        scratch_shapes=scratch,
        compiler_params=pltpu.CompilerParams(
            collective_id=0, has_side_effects=True, vmem_limit_bytes=62 * 1024 * 1024
        ),
    )
    return call, n_small


def solution(mesh):
    mesh_shape = dict(mesh.shape)

    def local(
        activations,
        norm_gain,
        query_weight,
        key_weight,
        value_weight,
        gate_weight,
        out_weight,
        mlp_gain,
        up_weight,
        down_weight,
    ):
        shapes = {
            "activations": activations.shape,
            "query_weight": query_weight.shape,
            "up_weight": up_weight.shape,
        }
        call, n_small = build(mesh_shape, shapes)
        small = (query_weight, key_weight, value_weight, gate_weight)
        if n_small == 1:
            small = (jnp.concatenate(small, axis=1),)
        cosine, sine, decay = tables(query_weight.shape[1])
        return call(
            activations,
            *small,
            out_weight,
            up_weight,
            down_weight,
            norm_gain.reshape(1, -1),
            mlp_gain.reshape(1, -1),
            jnp.asarray(cosine),
            jnp.asarray(sine),
            jnp.asarray(decay),
        )

    in_specs = (
        P(("rep", "fs"), "tp"),
        P(),
        P("fs", "tp"),
        P("fs", "tp"),
        P("fs", "tp"),
        P("fs", "tp"),
        P("tp", "fs"),
        P(),
        P("fs", "tp"),
        P("tp", "fs"),
    )
    return jax.shard_map(
        local, mesh=mesh, in_specs=in_specs, out_specs=P(("rep", "fs"), "tp"), check_vma=False
    )
```

profile of v0, /device:TPU:12, one launch (start us, length us, event | category | flops | bytes accessed | tf_op | source)
XLA Modules:
  0.0 182.2 jit_solution(12587645884652238162)
XLA Ops:
  0.0 180.4 %layer.1 = bf16[384,512]{1,0:T(8,128)(2,1)} custom-call(bf16[384,512]{1,0:T(8,128)(2,1)} %refs_0_.1, bf16[512,128]{1,0:T(8,128)(2,1)} %refs_1_.1, bf16[512,128]{1,0:T(8,128)(2,1)} %refs_2_.1, bf16[512,128]{1,0:T(8,128)(2,1)} %refs_3_.1, bf16[512,128]{1,0:T(8,128)(2,1)} %refs_4_.1, bf16[128,512]{1,0:T(8,128)(2,1)} %refs_5_.1, bf16[512,2048]{1,0:T(8,128)(2,1)} %refs_6_.1, ...), custom_call_target="tpu_custom_call" | custom-call | tf_op jit(solution)/shard_map/layer/pallas_call | solution.py:698
  180.4 1.8 copy.15
where the time goes:
time: 183 us; the launch traced here: 182 us
  Pallas kernels  180 us (98%)
    pallas_call x1, Pallas kernels, local(): call(activations, *small, out_weight, up_weight, down_weight, norm_gain.r...  180 us

commit v1 on v0

--- a/solution.py
+++ b/solution.py
@@ -66,7 +66,7 @@
         plan.take(1),
         plan.take(1),
         plan.take(1),
-        plan.take(1),
+        plan.take(R),
         plan.take(1),
         plan.take(n_small),
     )
@@ -82,14 +82,18 @@
     om_send, om_recv = plan.take((T - 1) * Q), plan.take(T * Q)
 
     class Stream:
-        def __init__(self):
-            self.zs, self.zf, self.zr = plan.take(max(F, 3)), plan.take(F), plan.take(F)
-            self.ys, self.yr = plan.take(F * R), plan.take(F * R)
-
-    qkv_stream, out_stream, up_stream, down_stream = Stream(), Stream(), Stream(), Stream()
-    ps, pr = plan.take(2 * F), plan.take(2 * F)
-    xs, xr = plan.take(2 * F), plan.take(2 * max(X - 1, 1) * Q)
-    fz_s, fz_r = plan.take(Q), plan.take(Q)
+        def __init__(self, chunks, line):
+            self.chunks, self.line = chunks, line
+            self.zs, self.zf, self.zr = (plan.take(3 * chunks), plan.take(F * chunks), plan.take(F * chunks))
+            self.ys, self.yr = plan.take(F * R * chunks), plan.take(F * R * chunks)
+
+    qkv_stream, out_stream = Stream(2, True), Stream(1, True)
+    up_stream, down_stream = Stream(2, False), Stream(2, False)
+    U = R if (dep // R) % 128 == 0 else 1
+    uc = dep // U
+    ps, pr = plan.take(2 * F * U), plan.take(2 * F * U)
+    xs, xr = plan.take(2 * F * U), plan.take(2 * max(X - 1, 1) * Q * U)
+    fz_s, fz_r = plan.take(Q * U), plan.take(Q * U)
 
     def kernel(*refs):
         act = refs[0]
@@ -161,29 +165,43 @@
         def ret_block(j, s):
             return ret.at[s, pl.ds(j * SEQ_LEN, SEQ_LEN), :]
 
-        def qkv_part(s, part):
-            rows = dep // R
-            return wbuf.at[span(s * dep + part * rows, rows, rows), :]
-
-        def out_part(s, part):
-            rows = hw // R
-            return og.at[s, span(part * rows, rows, rows), :]
-
-        def up_part(s, part):
-            rows = dep // R
-            return upb.at[span(s * dep + part * rows, rows, rows), :]
-
-        def down_part(s, part):
-            rows = hid // R
-            return dnb.at[s, span(part * rows, rows, rows), :]
-
-        def up_own(half):
-            rows = dep // R
-            return up_w.at[span(r * rows, rows, rows), span(half * hid, hid, hid)]
-
-        def down_own(half):
-            rows = hid // R
-            return down_w.at[span(half * hid + r * rows, rows, rows), :]
+        def rows_of(base, size, chunk, chunks):
+            rows = size // chunks
+            return span(base + chunk * rows, rows, rows)
+
+        def qkv_part(s, part, ch):
+            size = dep // R
+            return wbuf.at[rows_of(s * dep + part * size, size, ch, qkv_stream.chunks), :]
+
+        def out_part(s, part, ch):
+            size = hw // R
+            return og.at[s, rows_of(part * size, size, ch, out_stream.chunks), :]
+
+        def up_part(s, part, ch):
+            size = dep // R
+            return upb.at[rows_of(s * dep + part * size, size, ch, up_stream.chunks), :]
+
+        def down_part(s, part, ch):
+            if U > 1:
+                return dnb.at[s, part, rows_of(0, hid, ch, down_stream.chunks), :]
+            size = hid // R
+            return dnb.at[s, 0, rows_of(part * size, size, ch, down_stream.chunks), :]
+
+        def qkv_own(half, ch):
+            return qkv_part(f, r, ch)
+
+        def out_own(half, ch):
+            return out_part(f, r, ch)
+
+        def up_own(half, ch):
+            size = dep // R
+            return up_w.at[rows_of(r * size, size, ch, up_stream.chunks), span(half * hid, hid, hid)]
+
+        def down_own(half, ch):
+            if U > 1:
+                return down_w.at[rows_of(half * hid, hid, ch, down_stream.chunks), span(r * uc, uc, uc)]
+            size = hid // R
+            return down_w.at[rows_of(half * hid + r * size, size, ch, down_stream.chunks), :]
 
         def spread_copies(sp, block, source):
             first = [remote(source, block(t), sp.send, sp.recv + t, tp=sib)]
@@ -216,59 +234,89 @@
             for j in range(1, X):
                 relay_copy(sp, block, j).wait_send()
 
-        def y_copy(st, part, s, q):
-            return remote(
-                part(s, r), part(s, r), st.ys + s * R + q, st.yr + s * R + r, rep=(r + q) % R
-            )
-
-        def y_start(st, part, s):
-            for q in range(1, R):
-                y_copy(st, part, s, q).start()
+        deep = h * (f - HF) + (1 - h) * (HF - 1 - f)
+
+        def y_copy(st, part, s, ch, q):
+            block = part(s, r, ch)
+            base = (s * R + q) * st.chunks + ch
+            return remote(block, block, st.ys + base, st.yr + (s * R + r) * st.chunks + ch, rep=(r + q) % R)
 
         def y_wait(st, part, s):
             for q in range(1, R):
                 other = (r + R - q) % R
-                remote(
-                    part(s, other), part(s, other), st.ys, st.yr + s * R + other, rep=other
-                ).wait_recv()
-
-        def z_wait(st, part, s):
-            remote(part(s, r), part(s, r), st.zs, st.zr + s, fs=s).wait_recv()
-
-        def direct_copy(st, part, k):
-            return remote(part(f, r), part(f, r), st.zs + k, st.zr + f, fs=order(k))
-
-        def own_copies(st, part, own):
-            return (
-                remote(own(1 - h), part(f, r), st.zs, st.zr + f, fs=HF - h),
-                remote(own(h), part(f, r), st.zs + 1, st.zr + f, fs=(f + 1) % F),
-                remote(own(h), part(f, r), st.zs + 2, st.zr + f, fs=(f + F - 1) % F),
-            )
-
-        def own_do(st, part, own, what):
-            across, onward, back = own_copies(st, part, own)
-            what(across)
-
-            @pl.when(f % HF != HF - 1)
+                for ch in range(st.chunks):
+                    block = part(s, other, ch)
+                    remote(
+                        block, block, st.ys, st.yr + (s * R + other) * st.chunks + ch, rep=other
+                    ).wait_recv()
+
+        def z_wait(st, part, s, ch):
+            block = part(s, r, ch)
+            remote(block, block, st.zs, st.zr + s * st.chunks + ch, fs=s).wait_recv()
+
+        def along(st, part, own, what):
+            size = F if st.line else HF
+            for ch in range(st.chunks):
+                source, target, arrived = own(h, ch), part(f, r, ch), st.zr + f * st.chunks + ch
+
+                @pl.when(f % size != size - 1)
+                def _():
+                    what(remote(source, target, st.zs + ch, arrived, fs=(f + 1) % F))
+
+                @pl.when(f % size != 0)
+                def _():
+                    what(remote(source, target, st.zs + st.chunks + ch, arrived, fs=(f + F - 1) % F))
+
+        def across(st, part, own, what):
+            for ch in range(st.chunks):
+                what(
+                    remote(
+                        own(1 - h, ch),
+                        part(f, r, ch),
+                        st.zs + 2 * st.chunks + ch,
+                        st.zr + f * st.chunks + ch,
+                        fs=HF - h,
+                    )
+                )
+
+        def forward(st, part, s, ch, what):
+            after = f + 2 * ((f - s + F) // F) - 1
+            size = F if st.line else HF
+
+            @pl.when((after + size) // size - 1 == (0 if st.line else h))
             def _():
-                what(onward)
-
-            @pl.when(f % HF != 0)
-            def _():
-                what(back)
-
-        def forward_do(st, part, s, what):
-            after = f + 2 * ((f - s + F) // F) - 1
-
-            @pl.when((after + HF) // HF - 1 == h)
-            def _():
-                what(remote(part(s, r), part(s, r), st.zf + s, st.zr + s, fs=(after + F) % F))
+                block = part(s, r, ch)
+                what(
+                    remote(
+                        block,
+                        block,
+                        st.zf + s * st.chunks + ch,
+                        st.zr + s * st.chunks + ch,
+                        fs=(after + F) % F,
+                    )
+                )
+
+        def start(copy):
+            copy.start()
+
+        def leave(copy):
+            copy.wait_send()
 
         def pass_on(st, part, k):
             s = order(k)
-            z_wait(st, part, s)
-            forward_do(st, part, s, lambda copy: copy.start())
-            y_start(st, part, s)
+            for ch in range(st.chunks):
+                z_wait(st, part, s, ch)
+                forward(st, part, s, ch, start)
+                for q in range(1, R):
+                    y_copy(st, part, s, ch, q).start()
+
+        def pass_range(st, part, first, last):
+            def body(k, carry):
+                pass_on(st, part, k)
+                return carry
+
+            if last > first:
+                lax.fori_loop(first, last, body, 0)
 
         head0 = t * local_heads
         loads = [local(act, act_block(t), L_ACT)]
@@ -277,7 +325,10 @@
         loads.append(local(out_w, og.at[f], L_OUT))
         loads.append(local(decay_all.at[pl.ds(head0, local_heads)], decay, L_DECAY))
         loads.append(local(up_w.at[:, span(h * hid, hid, hid)], upb.at[span(f * dep, dep, dep), :], L_UP))
-        loads.append(local(down_w.at[span(h * hid, hid, hid), :], dnb.at[f], L_DOWN))
+        for u in range(U):
+            loads.append(
+                local(down_w.at[span(h * hid, hid, hid), u * uc : (u + 1) * uc], dnb.at[f, u], L_DOWN + u)
+            )
         for copy in loads:
             copy.start()
 
@@ -293,15 +344,17 @@
         spread_start(act_spread, act_block, act)
         for i in range(n_small):
             loads[1 + i].wait()
-        for k in range(1, F):
-            direct_copy(qkv_stream, qkv_part, k).start()
+        along(qkv_stream, qkv_part, qkv_own, start)
         loads[1 + n_small].wait()
-        for k in range(1, F):
-            direct_copy(out_stream, out_part, k).start()
-        own_do(up_stream, up_part, up_own, lambda copy: copy.start())
+        along(out_stream, out_part, out_own, start)
+        pass_on(qkv_stream, qkv_part, 1)
+        pass_on(out_stream, out_part, 1)
+
+        @pl.when(deep > 0)
+        def _():
+            along(up_stream, up_part, up_own, start)
+
         loads[0].wait()
-        for copy in loads[2 + n_small :]:
-            copy.wait()
 
         spread_relay(act_spread, act_block)
         spread_finish(act_spread, act_block)
@@ -334,33 +387,32 @@
         project(0)
 
         def small_on(k, carry):
-            s = order(k)
-            z_wait(qkv_stream, qkv_part, s)
-            y_start(qkv_stream, qkv_part, s)
+            pass_on(qkv_stream, qkv_part, k)
+            pass_on(out_stream, out_part, k)
             return carry
 
-        lax.fori_loop(1, F, small_on, 0)
-
-        def out_on(k, carry):
-            s = order(k)
-            z_wait(out_stream, out_part, s)
-            y_start(out_stream, out_part, s)
-            return carry
-
-        lax.fori_loop(1, F, out_on, 0)
+        lax.fori_loop(2, F, small_on, 0)
+
+        def own_weights(st, part, own):
+            @pl.when(deep == 0)
+            def _():
+                along(st, part, own, start)
+
+            @pl.when(deep > 0)
+            def _():
+                along(st, part, own, leave)
+
+            across(st, part, own, start)
+
+        own_weights(up_stream, up_part, up_own)
 
         def small_use(k, carry):
             y_wait(qkv_stream, qkv_part, order(k))
             project(k)
-            return carry
-
-        lax.fori_loop(1, F, small_use, 0)
-
-        def out_take(k, carry):
             y_wait(out_stream, out_part, order(k))
             return carry
 
-        lax.fori_loop(1, F, out_take, 0)
+        lax.fori_loop(1, F, small_use, 0)
 
         def om_copy(j, i):
             to = (t + j) % T
@@ -392,6 +444,7 @@
                 total += of_head(jnp.broadcast_to(mean, values.shape), i)
             return total
 
+        loads[2 + n_small].wait()
         for j in range(seqs):
             rows = pl.ds(j * SEQ_LEN, SEQ_LEN)
             raw = proj[rows, : 2 * hw]
@@ -417,7 +470,8 @@
             block = functools.partial(ret_block, j)
             spread_start(ret_spread[j], block, block(t))
 
-        pass_on(up_stream, up_part, 1)
+        third = (F + 1) // 3
+        pass_range(up_stream, up_part, 1, 1 + third)
 
         for j in range(1, T):
             s = (t + T - j) % T
@@ -443,16 +497,7 @@
         spread_start(mid_spread[0], mid_own, mid_own(t))
         to_partner = remote(mid_own(t), mid_other(t), mid_z[0], mid_z[1], fs=partner)
         to_partner.start()
-        own_do(down_stream, down_part, down_own, lambda copy: copy.start())
-
-        def up_on(k, carry):
-            pass_on(up_stream, up_part, k)
-            return carry
-
-        lax.fori_loop(2, F, up_on, 0)
-
-        spread_relay(mid_spread[0], mid_own)
-        spread_finish(mid_spread[0], mid_own)
+        pass_range(up_stream, up_part, 1 + third, F - third)
 
         def norm_second(g):
             def body(i, carry):
@@ -462,9 +507,18 @@
 
             lax.fori_loop(0, n // step, body, 0)
 
-        norm_second(0)
         to_partner.wait_recv()
         spread_start(mid_spread[1], mid_other, mid_other(t))
+        spread_relay(mid_spread[0], mid_own)
+        spread_finish(mid_spread[0], mid_own)
+        norm_second(0)
+
+        @pl.when(deep > 0)
+        def _():
+            along(down_stream, down_part, down_own, start)
+
+        pass_range(up_stream, up_part, F - third, F)
+        own_weights(down_stream, down_part, down_own)
         spread_relay(mid_spread[1], mid_other)
         spread_finish(mid_spread[1], mid_other)
         norm_second(1)
@@ -482,6 +536,7 @@
                 else:
                     acc[g] += part
 
+        loads[3 + n_small].wait()
         raise_by(0)
 
         def up_use(k, carry):
@@ -494,89 +549,117 @@
             kept = jnp.maximum(acc[g], 0.0)
             hidden[g] = (kept * kept).astype(BF16)
 
-        def where_to(k):
-            s = order(k)
-            return s, s // Q, s % Q
-
-        def lower(k):
-            s, td, i = where_to(k)
-            xd, cd = td // 2, td % 2
-            for g in (1, 0):
-                pf[g] = jnp.dot(hidden[g], dnb[s], preferred_element_type=F32)
-
-                @pl.when(c != cd)
-                def _():
-                    pbuf[s, g] = pf[g].astype(BF16)
-                    remote(
-                        pbuf.at[s, g], srecv.at[s, g], ps + 2 * s + g, pr + 2 * s + g, tp=sib
-                    ).start()
-
-            @pl.when(c == cd)
-            def _():
-                for g in (1, 0):
-                    remote(
-                        pbuf.at[s, g], srecv.at[s, g], ps + 2 * s + g, pr + 2 * s + g, tp=sib
-                    ).wait_recv()
-                    total = pf[g] + srecv[s, g].astype(F32)
-
-                    @pl.when(x == xd)
-                    def _():
-                        tot[g, i] = total
-
-                    @pl.when(x != xd)
-                    def _():
-                        pbuf[s, g] = total.astype(BF16)
-                        x_copy(s, g).start()
-
-        def x_copy(s, g):
+        def p_copy(s, u, g):
+            i = (s * U + u) * 2 + g
+            return remote(pbuf.at[s, u, g], srecv.at[s, u, g], ps + i, pr + i, tp=sib)
+
+        def x_copy(s, u, g):
             td, i = s // Q, s % Q
             away = (x + X - td // 2) % X
             slot = (away + X - 1) % X % max(X - 1, 1)
             return remote(
-                pbuf.at[s, g],
-                xrecv.at[slot, g, i],
-                xs + 2 * s + g,
-                xr + (slot * 2 + g) * Q + i,
+                pbuf.at[s, u, g],
+                xrecv.at[slot, g, i, u],
+                xs + (s * U + u) * 2 + g,
+                xr + ((slot * 2 + g) * Q + i) * U + u,
                 tp=(td // 2) * 2 + c,
             )
 
-        def z_copy(i):
-            return remote(zsnd.at[i], zrecv.at[i], fz_s + i, fz_r + i, fs=partner)
-
-        def settle(k):
-            s, td, i = where_to(k)
+        def z_copy(i, u):
+            return remote(zsnd.at[i, u], zrecv.at[i, u], fz_s + i * U + u, fz_r + i * U + u, fs=partner)
+
+        def unit(u):
+            return (r + u) % U
+
+        def lower(k, u):
+            s = order(k)
+            u = unit(u)
+            td, i = s // Q, s % Q
+            xd, cd = td // 2, td % 2
+            for g in (1, 0):
+                pf[g] = jnp.dot(hidden[g], dnb[s, u], preferred_element_type=F32)
+
+                @pl.when(c != cd)
+                def _():
+                    pbuf[s, u, g] = pf[g].astype(BF16)
+                    p_copy(s, u, g).start()
+
+            @pl.when(c == cd)
+            def _():
+                for g in (1, 0):
+                    p_copy(s, u, g).wait_recv()
+                    total = pf[g] + srecv[s, u, g].astype(F32)
+
+                    @pl.when(x == xd)
+                    def _():
+                        tot[g, i, u] = total
+
+                    @pl.when(x != xd)
+                    def _():
+                        pbuf[s, u, g] = total.astype(BF16)
+                        x_copy(s, u, g).start()
+
+        def settle(k, u):
+            s = order(k)
+            u = unit(u)
+            td, i = s // Q, s % Q
 
             @pl.when(td == t)
             def _():
                 for g in (1, 0):
-                    total = tot[g, i]
+                    total = tot[g, i, u]
                     for slot in range(X - 1):
-                        block = xrecv.at[slot, g, i]
-                        remote(block, block, xs, xr + (slot * 2 + g) * Q + i, tp=sib).wait_recv()
-                        total += xrecv[slot, g, i].astype(F32)
+                        block = xrecv.at[slot, g, i, u]
+                        remote(block, block, xs, xr + ((slot * 2 + g) * Q + i) * U + u, tp=sib).wait_recv()
+                        total += xrecv[slot, g, i, u].astype(F32)
                     if g == 1:
-                        zsnd[i] = total.astype(BF16)
-                        z_copy(i).start()
+                        zsnd[i, u] = total.astype(BF16)
+                        z_copy(i, u).start()
                     else:
-                        tot[0, i] = total
-
-        lower(0)
+                        tot[0, i, u] = total
+
+        pass_on(down_stream, down_part, 1)
+        for copy in loads[4 + n_small :]:
+            copy.wait()
+        for u in range(U):
+            lower(0, u)
+        if U > 1:
+            lower(1, 0)
 
         def down_use(k, carry):
             pass_on(down_stream, down_part, k)
-            y_wait(down_stream, down_part, order(k))
-            lower(k)
-            settle(k - 1)
+            y_wait(down_stream, down_part, order(k - 1))
+            if U > 1:
+                settle(k - 2, 0)
+                for u in range(1, U):
+                    lower(k - 1, u)
+                    settle(k - 2, u)
+                lower(k, 0)
+            else:
+                lower(k - 1, 0)
+                settle(k - 2, 0)
             return carry
 
-        lax.fori_loop(1, F, down_use, 0)
-        settle(F - 1)
+        lax.fori_loop(2, F, down_use, 0)
+        settle(F - 2, 0)
+        y_wait(down_stream, down_part, order(F - 1))
+        if U > 1:
+            settle(F - 1, 0)
+            for u in range(1, U):
+                lower(F - 1, u)
+                settle(F - 2, u)
+                settle(F - 1, u)
+        else:
+            lower(F - 1, 0)
+            settle(F - 1, 0)
         for i in range(Q):
-            z_copy(i).wait_recv()
-            columns = span(t * dc + i * dep, dep, dep)
-            result[:, i * dep : (i + 1) * dep] = (
-                mid[0, :, columns].astype(F32) + (tot[0, i] + zrecv[i].astype(F32))
-            ).astype(BF16)
+            for u in range(U):
+                z_copy(i, u).wait_recv()
+                base = i * dep + u * uc
+                columns = span(t * dc + base, uc, uc)
+                result[:, base : base + uc] = (
+                    mid[0, :, columns].astype(F32) + (tot[0, i, u] + zrecv[i, u].astype(F32))
+                ).astype(BF16)
 
         spread_drain(act_spread, act_block, act)
         for j in range(seqs):
@@ -589,41 +672,48 @@
             for i in range(Q):
                 om_copy(j, i).wait_send()
         for i in range(Q):
-            z_copy(i).wait_send()
-        own_do(up_stream, up_part, up_own, lambda copy: copy.wait_send())
-        own_do(down_stream, down_part, down_own, lambda copy: copy.wait_send())
+            for u in range(U):
+                z_copy(i, u).wait_send()
+        streams = (
+            (qkv_stream, qkv_part, qkv_own),
+            (out_stream, out_part, out_own),
+            (up_stream, up_part, up_own),
+            (down_stream, down_part, down_own),
+        )
+        for st, part, own in streams:
+            if st.line:
+                along(st, part, own, leave)
+            else:
+
+                @pl.when(deep == 0)
+                def _():
+                    along(st, part, own, leave)
+
+                across(st, part, own, leave)
 
         def sent(k, carry):
             s = order(k)
-            direct_copy(qkv_stream, qkv_part, k).wait_send()
-            direct_copy(out_stream, out_part, k).wait_send()
-            forward_do(up_stream, up_part, s, lambda copy: copy.wait_send())
-            forward_do(down_stream, down_part, s, lambda copy: copy.wait_send())
-            for st, part in (
-                (qkv_stream, qkv_part),
-                (out_stream, out_part),
-                (up_stream, up_part),
-                (down_stream, down_part),
-            ):
-                for q in range(1, R):
-                    y_copy(st, part, s, q).wait_send()
+            for st, part, own in streams:
+                for ch in range(st.chunks):
+                    forward(st, part, s, ch, leave)
+                    for q in range(1, R):
+                        y_copy(st, part, s, ch, q).wait_send()
             return carry
 
         lax.fori_loop(1, F, sent, 0)
 
-        def summed(k, carry):
-            s, td, i = where_to(k)
-            for g in range(2):
-
-                @pl.when(c != td % 2)
-                def _():
-                    remote(
-                        pbuf.at[s, g], srecv.at[s, g], ps + 2 * s + g, pr + 2 * s + g, tp=sib
-                    ).wait_send()
-
-                @pl.when((c == td % 2) & (x != td // 2))
-                def _():
-                    x_copy(s, g).wait_send()
+        def summed(s, carry):
+            td = s // Q
+            for u in range(U):
+                for g in range(2):
+
+                    @pl.when(c != td % 2)
+                    def _():
+                        p_copy(s, u, g).wait_send()
+
+                    @pl.when((c == td % 2) & (x != td // 2))
+                    def _():
+                        x_copy(s, u, g).wait_send()
 
             return carry
 
@@ -642,16 +732,16 @@
         vmem((2, n, D), BF16),
         vmem((2, n, D), BF16),
         vmem((D, hid), BF16),
-        vmem((F, hid, dep), BF16),
+        vmem((F, U, hid, uc), BF16),
         vmem((2, n, hid), F32),
         vmem((2, n, hid), BF16),
-        vmem((2, n, dep), F32),
-        vmem((F, 2, n, dep), BF16),
-        vmem((F, 2, n, dep), BF16),
-        vmem((2, Q, n, dep), F32),
-        vmem((max(X - 1, 1), 2, Q, n, dep), BF16),
-        vmem((Q, n, dep), BF16),
-        vmem((Q, n, dep), BF16),
+        vmem((2, n, uc), F32),
+        vmem((F, U, 2, n, uc), BF16),
+        vmem((F, U, 2, n, uc), BF16),
+        vmem((2, Q, U, n, uc), F32),
+        vmem((max(X - 1, 1), 2, Q, U, n, uc), BF16),
+        vmem((Q, U, n, uc), BF16),
+        vmem((Q, U, n, uc), BF16),
         pltpu.SemaphoreType.DMA((plan.size,)),
     ]
     anywhere = pl.BlockSpec(memory_space=pl.ANY)

time: 183 us -> 150 us (0.82)
  Pallas kernels: 180 us -> 147 us
    pallas_call x1, Pallas kernels: 180 us -> 147 us  [local(): call(activations, *small, out_weight, up_weight, down_weight, norm_gain.r...]
where the time goes in v1:
time: 150 us; the launch traced here: 149 us
  Pallas kernels  147 us (98%)
  local copies, waits for them, and re-layouts  1.77 us (1%)
    pallas_call x1, Pallas kernels, local(): call(activations, *small, out_weight, up_weight, down_weight, norm_gain.r...  147 us

profile of v1, /device:TPU:12, one launch (start us, length us, event | category | flops | bytes accessed | tf_op | source)
XLA Modules:
  0.0 148.7 jit_solution(10701582853288810855)
XLA Ops:
  0.0 146.9 %layer.1 = bf16[384,512]{1,0:T(8,128)(2,1)} custom-call(bf16[384,512]{1,0:T(8,128)(2,1)} %refs_0_.1, bf16[512,128]{1,0:T(8,128)(2,1)} %refs_1_.1, bf16[512,128]{1,0:T(8,128)(2,1)} %refs_2_.1, bf16[512,128]{1,0:T(8,128)(2,1)} %refs_3_.1, bf16[512,128]{1,0:T(8,128)(2,1)} %refs_4_.1, bf16[128,512]{1,0:T(8,128)(2,1)} %refs_5_.1, bf16[512,2048]{1,0:T(8,128)(2,1)} %refs_6_.1, ...), custom_call_target="tpu_custom_call" | custom-call | tf_op jit(solution)/shard_map/layer/pallas_call | solution.py:788
  147.0 1.8 %copy.15 = bf16[384,512]{1,0:T(8,128)(2,1)} copy(bf16[384,512]{1,0:T(8,128)(2,1)} %layer.1) | data formatting | bytes 786432

commit v2 on v1

--- a/solution.py
+++ b/solution.py
@@ -38,6 +38,125 @@
     return cosine.astype(np.float32), sine.astype(np.float32), decay.astype(np.float32)
 
 
+NEAR_FOUR = {
+    ("begin",): (
+        ("ps", 1),
+        ("ps", 2),
+    ),
+    ("act",): (
+        ("alu", 0),
+    ),
+    ("proj", 1): (
+        ("acu", 0),
+        ("ps", 3),
+        ("alu", 1),
+        ("pu", 2, 1),
+        ("acu", 1),
+        ("ald", 0),
+        ("ald", 1),
+    ),
+    ("ret",): (
+        ("pu", 3, 0),
+        ("pu", 3, 1),
+        ("pu", 2, 0),
+    ),
+    ("m0",): (
+        ("pu", 1, 0),
+        ("pu", 1, 1),
+        ("acd", 0),
+    ),
+    ("tok",): (
+        ("acd", 1),
+    ),
+    ("raise", 0): (
+        ("pd", 2, 1),
+    ),
+    ("raise", 1): (
+        ("pd", 3, 1),
+    ),
+    ("raise", 2): (
+        ("pd", 1, 1),
+    ),
+    ("low", 0, 1): (
+        ("pd", 1, 0),
+        ("pd", 2, 0),
+        ("pd", 3, 0),
+    ),
+}
+DEEP_FOUR = {
+    ("begin",): (
+        ("ps", 1),
+        ("alu", 0),
+        ("alu", 1),
+        ("acu", 0),
+    ),
+    ("act",): (
+        ("acd", 1),
+        ("acu", 1),
+        ("ps", 2),
+    ),
+    ("proj", 2): (
+        ("ps", 3),
+        ("pu", 1, 0),
+    ),
+    ("ret",): (
+        ("pu", 1, 1),
+    ),
+    ("mid",): (
+        ("ald", 0),
+        ("ald", 1),
+        ("pd", 1, 0),
+        ("pd", 1, 1),
+        ("pu", 3, 0),
+        ("pu", 3, 1),
+    ),
+    ("tok",): (
+        ("pu", 2, 0),
+        ("pu", 2, 1),
+    ),
+    ("m1",): (
+        ("pd", 3, 1),
+        ("acd", 0),
+    ),
+    ("raise", 2): (
+        ("pd", 2, 1),
+    ),
+    ("low", 0, 1): (
+        ("pd", 2, 0),
+    ),
+    ("low", 2, 0): (
+        ("pd", 3, 0),
+    ),
+}
+
+
+def spread_moves(planes, chunks):
+    def every(name):
+        return tuple((name, k, ch) for k in range(1, planes) for ch in range(chunks))
+
+    def own(*names):
+        return tuple((name, ch) for name in names for ch in range(chunks))
+
+    return {
+        ("begin",): tuple(("ps", k) for k in range(1, planes)) + own("alu", "acu"),
+        ("mid",): every("pu") + own("ald", "acd"),
+        ("tok",): every("pd"),
+    }
+
+
+def chain(planes, units):
+    steps = [("begin",), ("act",)] + [("proj", k) for k in range(1, planes)]
+    steps += [("ret",), ("mid",), ("m0",), ("tok",), ("m1",)] + [("raise", k) for k in range(planes)]
+    pieces = [(k, u) for k in range(planes) for u in range(units)]
+    behind = 2 if units > 1 else 1
+    for i, piece in enumerate(pieces):
+        steps.append(("low", *piece))
+        if i >= behind:
+            steps.append(("set", *pieces[i - behind]))
+    steps += [("set", *piece) for piece in pieces[-behind:]]
+    return steps + [("end",)]
+
+
 class Plan:
     def __init__(self):
         self.size = 0
@@ -87,6 +206,7 @@
             self.zs, self.zf, self.zr = (plan.take(3 * chunks), plan.take(F * chunks), plan.take(F * chunks))
             self.ys, self.yr = plan.take(F * R * chunks), plan.take(F * R * chunks)
 
+    near_moves, deep_moves = (NEAR_FOUR, DEEP_FOUR) if F == 4 else (spread_moves(F, 2), spread_moves(F, 2))
     qkv_stream, out_stream = Stream(2, True), Stream(1, True)
     up_stream, down_stream = Stream(2, False), Stream(2, False)
     U = R if (dep // R) % 128 == 0 else 1
@@ -254,9 +374,9 @@
             block = part(s, r, ch)
             remote(block, block, st.zs, st.zr + s * st.chunks + ch, fs=s).wait_recv()
 
-        def along(st, part, own, what):
+        def along(st, part, own, what, chunks=None):
             size = F if st.line else HF
-            for ch in range(st.chunks):
+            for ch in range(st.chunks) if chunks is None else chunks:
                 source, target, arrived = own(h, ch), part(f, r, ch), st.zr + f * st.chunks + ch
 
                 @pl.when(f % size != size - 1)
@@ -267,8 +387,8 @@
                 def _():
                     what(remote(source, target, st.zs + st.chunks + ch, arrived, fs=(f + F - 1) % F))
 
-        def across(st, part, own, what):
-            for ch in range(st.chunks):
+        def across(st, part, own, what, chunks=None):
+            for ch in range(st.chunks) if chunks is None else chunks:
                 what(
                     remote(
                         own(1 - h, ch),
@@ -302,21 +422,13 @@
         def leave(copy):
             copy.wait_send()
 
-        def pass_on(st, part, k):
+        def pass_on(st, part, k, chunks=None):
             s = order(k)
-            for ch in range(st.chunks):
+            for ch in range(st.chunks) if chunks is None else chunks:
                 z_wait(st, part, s, ch)
                 forward(st, part, s, ch, start)
                 for q in range(1, R):
                     y_copy(st, part, s, ch, q).start()
-
-        def pass_range(st, part, first, last):
-            def body(k, carry):
-                pass_on(st, part, k)
-                return carry
-
-            if last > first:
-                lax.fori_loop(first, last, body, 0)
 
         head0 = t * local_heads
         loads = [local(act, act_block(t), L_ACT)]
@@ -341,23 +453,14 @@
             pl.semaphore_signal(barrier, inc=1, device_id={"rep": (r + j) % R}, device_id_type=MESH)
         pl.semaphore_wait(barrier, T + F + R - 3)
 
-        spread_start(act_spread, act_block, act)
-        for i in range(n_small):
-            loads[1 + i].wait()
-        along(qkv_stream, qkv_part, qkv_own, start)
-        loads[1 + n_small].wait()
-        along(out_stream, out_part, out_own, start)
-        pass_on(qkv_stream, qkv_part, 1)
-        pass_on(out_stream, out_part, 1)
-
-        @pl.when(deep > 0)
-        def _():
-            along(up_stream, up_part, up_own, start)
-
-        loads[0].wait()
-
-        spread_relay(act_spread, act_block)
-        spread_finish(act_spread, act_block)
+        def begin():
+            spread_start(act_spread, act_block, act)
+            for i in range(n_small):
+                loads[1 + i].wait()
+            along(qkv_stream, qkv_part, qkv_own, start)
+            loads[1 + n_small].wait()
+            along(out_stream, out_part, out_own, start)
+
         step = 64
 
         def norm_rows(source, gain, target):
@@ -370,7 +473,12 @@
             norm_rows(act_full[rows, :], gain1, normed.at[rows, :])
             return carry
 
-        lax.fori_loop(0, n // step, norm_first, 0)
+        def norm_act():
+            loads[0].wait()
+            spread_relay(act_spread, act_block)
+            spread_finish(act_spread, act_block)
+            lax.fori_loop(0, n // step, norm_first, 0)
+            project(0)
 
         def project(k):
             s = order(k)
@@ -379,40 +487,17 @@
                 wbuf[span(s * dep, dep, dep), :],
                 preferred_element_type=F32,
             )
-            if isinstance(k, int):
+            if k == 0:
                 proj[...] = part
             else:
                 proj[...] += part
 
-        project(0)
-
-        def small_on(k, carry):
-            pass_on(qkv_stream, qkv_part, k)
-            pass_on(out_stream, out_part, k)
-            return carry
-
-        lax.fori_loop(2, F, small_on, 0)
-
-        def own_weights(st, part, own):
-            @pl.when(deep == 0)
-            def _():
-                along(st, part, own, start)
-
-            @pl.when(deep > 0)
-            def _():
-                along(st, part, own, leave)
-
-            across(st, part, own, start)
-
-        own_weights(up_stream, up_part, up_own)
-
-        def small_use(k, carry):
+        def project_with(k):
             y_wait(qkv_stream, qkv_part, order(k))
             project(k)
             y_wait(out_stream, out_part, order(k))
-            return carry
-
-        lax.fori_loop(1, F, small_use, 0)
+            if k == F - 1:
+                om_start()
 
         def om_copy(j, i):
             to = (t + j) % T
@@ -424,11 +509,12 @@
                 tp=to,
             )
 
-        for j in range(1, T):
+        def om_start():
+            for j in range(1, T):
+                for i in range(Q):
+                    om_copy(j, i).start()
             for i in range(Q):
-                om_copy(j, i).start()
-        for i in range(Q):
-            om[i, span(t * hw, hw, hw), :] = og[t * Q + i]
+                om[i, span(t * hw, hw, hw), :] = og[t * Q + i]
 
         lane = lax.broadcasted_iota(jnp.int32, (SEQ_LEN, 2 * hw), 1)
         first_half = lane % HEAD_DIM < HEAD_DIM // 2
@@ -444,60 +530,59 @@
                 total += of_head(jnp.broadcast_to(mean, values.shape), i)
             return total
 
-        loads[2 + n_small].wait()
-        for j in range(seqs):
-            rows = pl.ds(j * SEQ_LEN, SEQ_LEN)
-            raw = proj[rows, : 2 * hw]
-            turned = jnp.where(
-                first_half,
-                pltpu.roll(raw, 2 * hw - HEAD_DIM // 2, 1),
-                pltpu.roll(raw, HEAD_DIM // 2, 1),
-            )
-            both = raw * cosine[...] + turned * sine[...]
-            query, key = both[:, :hw], both[:, hw:].astype(BF16)
-            value = proj[rows, 2 * hw : 3 * hw]
-            gate = proj[rows, 3 * hw :]
-            mixed = jnp.zeros((SEQ_LEN, hw), F32)
-            for i in range(local_heads):
-                scores = lax.dot_general(
-                    of_head(query, i).astype(BF16), key, (((1,), (1,)), ((), ())), preferred_element_type=F32
+        def retain():
+            loads[2 + n_small].wait()
+            for j in range(seqs):
+                rows = pl.ds(j * SEQ_LEN, SEQ_LEN)
+                raw = proj[rows, : 2 * hw]
+                turned = jnp.where(
+                    first_half,
+                    pltpu.roll(raw, 2 * hw - HEAD_DIM // 2, 1),
+                    pltpu.roll(raw, HEAD_DIM // 2, 1),
                 )
-                weights = (scores * decay[i]).astype(BF16)
-                mixed += jnp.dot(weights, of_head(value, i).astype(BF16), preferred_element_type=F32)
-            centred = mixed - head_mean(mixed)
-            spread_of = lax.rsqrt(head_mean(centred * centred) + EPSILON)
-            ret[t, rows, :] = (centred * spread_of * (gate * jax.nn.sigmoid(gate))).astype(BF16)
-            block = functools.partial(ret_block, j)
-            spread_start(ret_spread[j], block, block(t))
-
-        third = (F + 1) // 3
-        pass_range(up_stream, up_part, 1, 1 + third)
-
-        for j in range(1, T):
-            s = (t + T - j) % T
-            for i in range(Q):
-                block = om.at[i, span(s * hw, hw, hw), :]
-                remote(block, block, om_send, om_recv + s * Q + i, tp=s).wait_recv()
-        for j in range(seqs):
-            spread_relay(ret_spread[j], functools.partial(ret_block, j))
-        for j in range(seqs):
-            block = functools.partial(ret_block, j)
-            spread_finish(ret_spread[j], block)
-            rows = pl.ds(j * SEQ_LEN, SEQ_LEN)
-            for i in range(Q):
-                branch = jnp.zeros((SEQ_LEN, dep), F32)
-                for s in range(T):
-                    branch += jnp.dot(
-                        ret[s, rows, :], om[i, pl.ds(s * hw, hw), :], preferred_element_type=F32
+                both = raw * cosine[...] + turned * sine[...]
+                query, key = both[:, :hw], both[:, hw:].astype(BF16)
+                value = proj[rows, 2 * hw : 3 * hw]
+                gate = proj[rows, 3 * hw :]
+                mixed = jnp.zeros((SEQ_LEN, hw), F32)
+                for i in range(local_heads):
+                    scores = lax.dot_general(
+                        of_head(query, i).astype(BF16), key, (((1,), (1,)), ((), ())), preferred_element_type=F32
                     )
-                columns = span(t * dc + i * dep, dep, dep)
-                mid[0, rows, columns] = (act_full[rows, columns].astype(F32) + branch).astype(BF16)
+                    weights = (scores * decay[i]).astype(BF16)
+                    mixed += jnp.dot(weights, of_head(value, i).astype(BF16), preferred_element_type=F32)
+                centred = mixed - head_mean(mixed)
+                spread_of = lax.rsqrt(head_mean(centred * centred) + EPSILON)
+                ret[t, rows, :] = (centred * spread_of * (gate * jax.nn.sigmoid(gate))).astype(BF16)
+                block = functools.partial(ret_block, j)
+                spread_start(ret_spread[j], block, block(t))
+
         mid_own = functools.partial(mid_block, 0)
         mid_other = functools.partial(mid_block, 1)
-        spread_start(mid_spread[0], mid_own, mid_own(t))
         to_partner = remote(mid_own(t), mid_other(t), mid_z[0], mid_z[1], fs=partner)
-        to_partner.start()
-        pass_range(up_stream, up_part, 1 + third, F - third)
+
+        def middle():
+            for j in range(1, T):
+                s = (t + T - j) % T
+                for i in range(Q):
+                    block = om.at[i, span(s * hw, hw, hw), :]
+                    remote(block, block, om_send, om_recv + s * Q + i, tp=s).wait_recv()
+            for j in range(seqs):
+                spread_relay(ret_spread[j], functools.partial(ret_block, j))
+            for j in range(seqs):
+                block = functools.partial(ret_block, j)
+                spread_finish(ret_spread[j], block)
+                rows = pl.ds(j * SEQ_LEN, SEQ_LEN)
+                for i in range(Q):
+                    branch = jnp.zeros((SEQ_LEN, dep), F32)
+                    for s in range(T):
+                        branch += jnp.dot(
+                            ret[s, rows, :], om[i, pl.ds(s * hw, hw), :], preferred_element_type=F32
+                        )
+                    columns = span(t * dc + i * dep, dep, dep)
+                    mid[0, rows, columns] = (act_full[rows, columns].astype(F32) + branch).astype(BF16)
+            spread_start(mid_spread[0], mid_own, mid_own(t))
+            to_partner.start()
 
         def norm_second(g):
             def body(i, carry):
@@ -505,49 +590,34 @@
                 norm_rows(mid[g, rows, :], gain2, second.at[g, rows, :])
                 return carry
 
+            block = mid_other if g else mid_own
+            spread_relay(mid_spread[g], block)
+            spread_finish(mid_spread[g], block)
             lax.fori_loop(0, n // step, body, 0)
 
-        to_partner.wait_recv()
-        spread_start(mid_spread[1], mid_other, mid_other(t))
-        spread_relay(mid_spread[0], mid_own)
-        spread_finish(mid_spread[0], mid_own)
-        norm_second(0)
-
-        @pl.when(deep > 0)
-        def _():
-            along(down_stream, down_part, down_own, start)
-
-        pass_range(up_stream, up_part, F - third, F)
-        own_weights(down_stream, down_part, down_own)
-        spread_relay(mid_spread[1], mid_other)
-        spread_finish(mid_spread[1], mid_other)
-        norm_second(1)
+        def partner_rows():
+            to_partner.wait_recv()
+            spread_start(mid_spread[1], mid_other, mid_other(t))
 
         def raise_by(k):
             s = order(k)
+            if k == 0:
+                loads[3 + n_small].wait()
+            else:
+                y_wait(up_stream, up_part, s)
             for g in range(2):
                 part = jnp.dot(
                     second[g, :, span(s * dep, dep, dep)],
                     upb[span(s * dep, dep, dep), :],
                     preferred_element_type=F32,
                 )
-                if isinstance(k, int):
+                if k == 0:
                     acc[g] = part
+                elif k < F - 1:
+                    acc[g] += part
                 else:
-                    acc[g] += part
-
-        loads[3 + n_small].wait()
-        raise_by(0)
-
-        def up_use(k, carry):
-            y_wait(up_stream, up_part, order(k))
-            raise_by(k)
-            return carry
-
-        lax.fori_loop(1, F, up_use, 0)
-        for g in range(2):
-            kept = jnp.maximum(acc[g], 0.0)
-            hidden[g] = (kept * kept).astype(BF16)
+                    kept = jnp.maximum(acc[g] + part, 0.0)
+                    hidden[g] = (kept * kept).astype(BF16)
 
         def p_copy(s, u, g):
             i = (s * U + u) * 2 + g
@@ -573,6 +643,11 @@
 
         def lower(k, u):
             s = order(k)
+            if k == 0 and u == 0:
+                for copy in loads[4 + n_small :]:
+                    copy.wait()
+            if k > 0 and u == U - 1:
+                y_wait(down_stream, down_part, s)
             u = unit(u)
             td, i = s // Q, s % Q
             xd, cd = td // 2, td % 2
@@ -618,48 +693,55 @@
                     else:
                         tot[0, i, u] = total
 
-        pass_on(down_stream, down_part, 1)
-        for copy in loads[4 + n_small :]:
-            copy.wait()
-        for u in range(U):
-            lower(0, u)
-        if U > 1:
-            lower(1, 0)
-
-        def down_use(k, carry):
-            pass_on(down_stream, down_part, k)
-            y_wait(down_stream, down_part, order(k - 1))
-            if U > 1:
-                settle(k - 2, 0)
-                for u in range(1, U):
-                    lower(k - 1, u)
-                    settle(k - 2, u)
-                lower(k, 0)
-            else:
-                lower(k - 1, 0)
-                settle(k - 2, 0)
-            return carry
-
-        lax.fori_loop(2, F, down_use, 0)
-        settle(F - 2, 0)
-        y_wait(down_stream, down_part, order(F - 1))
-        if U > 1:
-            settle(F - 1, 0)
-            for u in range(1, U):
-                lower(F - 1, u)
-                settle(F - 2, u)
-                settle(F - 1, u)
-        else:
-            lower(F - 1, 0)
-            settle(F - 1, 0)
-        for i in range(Q):
-            for u in range(U):
-                z_copy(i, u).wait_recv()
-                base = i * dep + u * uc
-                columns = span(t * dc + base, uc, uc)
-                result[:, base : base + uc] = (
-                    mid[0, :, columns].astype(F32) + (tot[0, i, u] + zrecv[i, u].astype(F32))
-                ).astype(BF16)
+        def finish():
+            for i in range(Q):
+                for u in range(U):
+                    z_copy(i, u).wait_recv()
+                    base = i * dep + u * uc
+                    columns = span(t * dc + base, uc, uc)
+                    result[:, base : base + uc] = (
+                        mid[0, :, columns].astype(F32) + (tot[0, i, u] + zrecv[i, u].astype(F32))
+                    ).astype(BF16)
+
+        near = deep == 0
+        steps = {
+            "begin": begin,
+            "act": norm_act,
+            "proj": project_with,
+            "ret": retain,
+            "mid": middle,
+            "m0": lambda: norm_second(0),
+            "tok": partner_rows,
+            "m1": lambda: norm_second(1),
+            "raise": raise_by,
+            "low": lower,
+            "set": settle,
+            "end": finish,
+        }
+
+        def small_on(k):
+            pass_on(qkv_stream, qkv_part, k)
+            pass_on(out_stream, out_part, k)
+
+        moves = {
+            "ps": small_on,
+            "alu": lambda ch: along(up_stream, up_part, up_own, start, (ch,)),
+            "acu": lambda ch: across(up_stream, up_part, up_own, start, (ch,)),
+            "ald": lambda ch: along(down_stream, down_part, down_own, start, (ch,)),
+            "acd": lambda ch: across(down_stream, down_part, down_own, start, (ch,)),
+            "pu": lambda k, ch: pass_on(up_stream, up_part, k, (ch,)),
+            "pd": lambda k, ch: pass_on(down_stream, down_part, k, (ch,)),
+        }
+        for name, *place in chain(F, U):
+            steps[name](*place)
+            for here, table in ((near, near_moves), (deep > 0, deep_moves)):
+                todo = table.get((name, *place), ())
+                if todo:
+
+                    @pl.when(here)
+                    def _():
+                        for move, *which in todo:
+                            moves[move](*which)
 
         spread_drain(act_spread, act_block, act)
         for j in range(seqs):
@@ -681,14 +763,8 @@
             (down_stream, down_part, down_own),
         )
         for st, part, own in streams:
-            if st.line:
-                along(st, part, own, leave)
-            else:
-
-                @pl.when(deep == 0)
-                def _():
-                    along(st, part, own, leave)
-
+            along(st, part, own, leave)
+            if not st.line:
                 across(st, part, own, leave)
 
         def sent(k, carry):

time: 150 us -> 134 us (0.89); the launches traced: 149 us -> 134 us
  Pallas kernels: 147 us -> 132 us
    pallas_call x1, Pallas kernels: 147 us -> 132 us  [local(): call(activations, *small, out_weight, up_weight, down_weight, norm_gain.r...]
where the time goes in v2:
time: 134 us
  Pallas kernels  132 us (99%)
  local copies, waits for them, and re-layouts  1.77 us (1%)
    pallas_call x1, Pallas kernels, local(): call(activations, *small, out_weight, up_weight, down_weight, norm_gain.r...  132 us

profile of v2, /device:TPU:12, one launch (start us, length us, event | category | flops | bytes accessed | tf_op | source)
XLA Modules:
  0.0 134.2 jit_solution(4714940443173068293)
XLA Ops:
  0.0 132.5 %layer.1 = bf16[384,512]{1,0:T(8,128)(2,1)} custom-call(bf16[384,512]{1,0:T(8,128)(2,1)} %refs_0_.1, bf16[512,128]{1,0:T(8,128)(2,1)} %refs_1_.1, bf16[512,128]{1,0:T(8,128)(2,1)} %refs_2_.1, bf16[512,128]{1,0:T(8,128)(2,1)} %refs_3_.1, bf16[512,128]{1,0:T(8,128)(2,1)} %refs_4_.1, bf16[128,512]{1,0:T(8,128)(2,1)} %refs_5_.1, bf16[512,2048]{1,0:T(8,128)(2,1)} %refs_6_.1, ...), custom_call_target="tpu_custom_call" | custom-call | tf_op jit(solution)/shard_map/layer/pallas_call | solution.py:864
  132.5 1.8 %copy.15 = bf16[384,512]{1,0:T(8,128)(2,1)} copy(bf16[384,512]{1,0:T(8,128)(2,1)} %layer.1) | data formatting | bytes 786432

commit v3 on v2

--- a/solution.py
+++ b/solution.py
@@ -40,107 +40,144 @@
 
 NEAR_FOUR = {
     ("begin",): (
+        ("alu", 0),
+        ("ald", 3),
+        ("ps", 2),
+        ("acu", 1),
+    ),
+    ("act",): (
+        ("acu", 0),
         ("ps", 1),
-        ("ps", 2),
-    ),
-    ("act",): (
-        ("alu", 0),
+        ("ps", 3),
     ),
     ("proj", 1): (
-        ("acu", 0),
-        ("ps", 3),
+        ("acd", 3),
+        ("pu", 2, 1),
+    ),
+    ("proj", 2): (
         ("alu", 1),
-        ("pu", 2, 1),
-        ("acu", 1),
-        ("ald", 0),
-        ("ald", 1),
-    ),
-    ("ret",): (
+    ),
+    ("proj", 3): (
+        ("ald", 2),
+        ("pu", 1, 0),
+        ("pu", 1, 1),
+    ),
+    ("mid",): (
+        ("pu", 2, 0),
+        ("acd", 2),
+        ("acd", 1),
         ("pu", 3, 0),
         ("pu", 3, 1),
-        ("pu", 2, 0),
     ),
     ("m0",): (
-        ("pu", 1, 0),
-        ("pu", 1, 1),
+        ("ald", 1),
+    ),
+    ("tok",): (
+        ("pd", 2, 3),
         ("acd", 0),
-    ),
-    ("tok",): (
-        ("acd", 1),
+        ("pd", 1, 2),
+        ("pd", 1, 3),
+        ("pd", 1, 1),
+    ),
+    ("m1",): (
+        ("pd", 2, 2),
     ),
     ("raise", 0): (
         ("pd", 2, 1),
+        ("pd", 2, 0),
+        ("ald", 0),
     ),
     ("raise", 1): (
+        ("pd", 1, 0),
+    ),
+    ("raise", 3): (
+        ("pd", 3, 0),
         ("pd", 3, 1),
     ),
-    ("raise", 2): (
-        ("pd", 1, 1),
-    ),
-    ("low", 0, 1): (
-        ("pd", 1, 0),
-        ("pd", 2, 0),
-        ("pd", 3, 0),
+    ("low", 0, 0): (
+        ("pd", 3, 2),
+    ),
+    ("low", 1, 0): (
+        ("pd", 3, 3),
     ),
 }
 DEEP_FOUR = {
     ("begin",): (
-        ("ps", 1),
-        ("alu", 0),
-        ("alu", 1),
-        ("acu", 0),
-    ),
-    ("act",): (
-        ("acd", 1),
-        ("acu", 1),
-        ("ps", 2),
-    ),
-    ("proj", 2): (
-        ("ps", 3),
-        ("pu", 1, 0),
-    ),
-    ("ret",): (
-        ("pu", 1, 1),
-    ),
-    ("mid",): (
         ("ald", 0),
         ("ald", 1),
-        ("pd", 1, 0),
-        ("pd", 1, 1),
+        ("alu", 1),
+        ("alu", 0),
+        ("acu", 1),
+        ("ald", 2),
+        ("ald", 3),
+        ("ps", 1),
+        ("ps", 2),
+    ),
+    ("act",): (
+        ("ps", 3),
+    ),
+    ("proj", 2): (
+        ("acu", 0),
+    ),
+    ("proj", 3): (
+        ("pu", 1, 1),
+    ),
+    ("ret",): (
+        ("pd", 1, 2),
+        ("pd", 1, 3),
+        ("acd", 2),
+        ("pu", 1, 0),
+    ),
+    ("mid",): (
+        ("pu", 2, 0),
+        ("pu", 2, 1),
+    ),
+    ("tok",): (
+        ("acd", 3),
         ("pu", 3, 0),
         ("pu", 3, 1),
-    ),
-    ("tok",): (
-        ("pu", 2, 0),
-        ("pu", 2, 1),
+        ("acd", 0),
     ),
     ("m1",): (
-        ("pd", 3, 1),
-        ("acd", 0),
-    ),
-    ("raise", 2): (
-        ("pd", 2, 1),
+        ("pd", 1, 1),
+    ),
+    ("raise", 0): (
+        ("acd", 1),
+        ("pd", 2, 3),
+    ),
+    ("raise", 1): (
+        ("pd", 2, 2),
+    ),
+    ("low", 0, 0): (
+        ("pd", 1, 0),
     ),
     ("low", 0, 1): (
         ("pd", 2, 0),
+        ("pd", 2, 1),
+    ),
+    ("low", 1, 0): (
+        ("pd", 3, 0),
     ),
     ("low", 2, 0): (
-        ("pd", 3, 0),
+        ("pd", 3, 1),
+    ),
+    ("set", 0, 1): (
+        ("pd", 3, 2),
+    ),
+    ("low", 2, 1): (
+        ("pd", 3, 3),
     ),
 }
 
-
-def spread_moves(planes, chunks):
-    def every(name):
-        return tuple((name, k, ch) for k in range(1, planes) for ch in range(chunks))
-
-    def own(*names):
-        return tuple((name, ch) for name in names for ch in range(chunks))
-
+DEEP_COLUMNS = (0, 2, 1, 3)
+
+
+def spread_moves(planes):
+    others = range(1, planes)
     return {
-        ("begin",): tuple(("ps", k) for k in range(1, planes)) + own("alu", "acu"),
-        ("mid",): every("pu") + own("ald", "acd"),
-        ("tok",): every("pd"),
+        ("begin",): tuple(("ps", k) for k in others) + (("alu", 0), ("acu", 0)),
+        ("mid",): tuple(("pu", k, 0) for k in others) + (("ald", 0), ("acd", 0)),
+        ("tok",): tuple(("pd", k, 0) for k in others),
     }
 
 
@@ -150,6 +187,8 @@
     pieces = [(k, u) for k in range(planes) for u in range(units)]
     behind = 2 if units > 1 else 1
     for i, piece in enumerate(pieces):
+        if i == len(pieces) - 1:
+            steps.append(("left",))
         steps.append(("low", *piece))
         if i >= behind:
             steps.append(("set", *pieces[i - behind]))
@@ -206,9 +245,10 @@
             self.zs, self.zf, self.zr = (plan.take(3 * chunks), plan.take(F * chunks), plan.take(F * chunks))
             self.ys, self.yr = plan.take(F * R * chunks), plan.take(F * R * chunks)
 
-    near_moves, deep_moves = (NEAR_FOUR, DEEP_FOUR) if F == 4 else (spread_moves(F, 2), spread_moves(F, 2))
+    near_moves, deep_moves = (NEAR_FOUR, DEEP_FOUR) if F == 4 else (spread_moves(F), spread_moves(F))
+    up_chunks, down_chunks = (2, 4) if F == 4 else (1, 1)
     qkv_stream, out_stream = Stream(2, True), Stream(1, True)
-    up_stream, down_stream = Stream(2, False), Stream(2, False)
+    up_stream, down_stream = Stream(up_chunks, False), Stream(down_chunks, False)
     U = R if (dep // R) % 128 == 0 else 1
     uc = dep // U
     ps, pr = plan.take(2 * F * U), plan.take(2 * F * U)
@@ -641,8 +681,13 @@
         def unit(u):
             return (r + u) % U
 
+        def low_order(k):
+            if F != 4:
+                return order(k)
+            return (1 - deep) * order(k) + deep * order(DEEP_COLUMNS[k])
+
         def lower(k, u):
-            s = order(k)
+            s = low_order(k)
             if k == 0 and u == 0:
                 for copy in loads[4 + n_small :]:
                     copy.wait()
@@ -675,7 +720,7 @@
                         x_copy(s, u, g).start()
 
         def settle(k, u):
-            s = order(k)
+            s = low_order(k)
             u = unit(u)
             td, i = s // Q, s % Q
 
@@ -703,6 +748,72 @@
                         mid[0, :, columns].astype(F32) + (tot[0, i, u] + zrecv[i, u].astype(F32))
                     ).astype(BF16)
 
+        streams = (
+            (qkv_stream, qkv_part, qkv_own),
+            (out_stream, out_part, out_own),
+            (up_stream, up_part, up_own),
+            (down_stream, down_part, down_own),
+        )
+
+        def passed(st, part, k):
+            s = order(k)
+            for ch in range(st.chunks):
+                forward(st, part, s, ch, leave)
+                for q in range(1, R):
+                    y_copy(st, part, s, ch, q).wait_send()
+
+        def summed(k):
+            s = low_order(k)
+            td = s // Q
+            for u in range(U):
+                for g in range(2):
+
+                    @pl.when(c != td % 2)
+                    def _():
+                        p_copy(s, u, g).wait_send()
+
+                    @pl.when((c == td % 2) & (x != td // 2))
+                    def _():
+                        x_copy(s, u, g).wait_send()
+
+        def early_left():
+            spread_drain(act_spread, act_block, act)
+            for j in range(seqs):
+                block = functools.partial(ret_block, j)
+                spread_drain(ret_spread[j], block, block(t))
+            spread_drain(mid_spread[0], mid_own, mid_own(t))
+            spread_drain(mid_spread[1], mid_other, mid_other(t))
+            to_partner.wait_send()
+            for j in range(1, T):
+                for i in range(Q):
+                    om_copy(j, i).wait_send()
+            for st, part, own in streams:
+                along(st, part, own, leave)
+                if not st.line:
+                    across(st, part, own, leave)
+
+            def sent(k, carry):
+                for st, part, own in streams[:3]:
+                    passed(st, part, k)
+                return carry
+
+            def sent_down(k, carry):
+                passed(down_stream, down_part, k)
+                return carry
+
+            lax.fori_loop(1, F, sent, 0)
+            lax.fori_loop(1, F - 1, sent_down, 0)
+            for k in range(F - 2):
+                summed(k)
+
+        def late_left():
+            passed(down_stream, down_part, F - 1)
+            for k in range(F - 2, F):
+                summed(k)
+            for i in range(Q):
+                for u in range(U):
+                    z_copy(i, u).wait_send()
+
         near = deep == 0
         steps = {
             "begin": begin,
@@ -716,6 +827,7 @@
             "raise": raise_by,
             "low": lower,
             "set": settle,
+            "left": early_left,
             "end": finish,
         }
 
@@ -743,57 +855,7 @@
                         for move, *which in todo:
                             moves[move](*which)
 
-        spread_drain(act_spread, act_block, act)
-        for j in range(seqs):
-            block = functools.partial(ret_block, j)
-            spread_drain(ret_spread[j], block, block(t))
-        spread_drain(mid_spread[0], mid_own, mid_own(t))
-        spread_drain(mid_spread[1], mid_other, mid_other(t))
-        to_partner.wait_send()
-        for j in range(1, T):
-            for i in range(Q):
-                om_copy(j, i).wait_send()
-        for i in range(Q):
-            for u in range(U):
-                z_copy(i, u).wait_send()
-        streams = (
-            (qkv_stream, qkv_part, qkv_own),
-            (out_stream, out_part, out_own),
-            (up_stream, up_part, up_own),
-            (down_stream, down_part, down_own),
-        )
-        for st, part, own in streams:
-            along(st, part, own, leave)
-            if not st.line:
-                across(st, part, own, leave)
-
-        def sent(k, carry):
-            s = order(k)
-            for st, part, own in streams:
-                for ch in range(st.chunks):
-                    forward(st, part, s, ch, leave)
-                    for q in range(1, R):
-                        y_copy(st, part, s, ch, q).wait_send()
-            return carry
-
-        lax.fori_loop(1, F, sent, 0)
-
-        def summed(s, carry):
-            td = s // Q
-            for u in range(U):
-                for g in range(2):
-
-                    @pl.when(c != td % 2)
-                    def _():
-                        p_copy(s, u, g).wait_send()
-
-                    @pl.when((c == td % 2) & (x != td // 2))
-                    def _():
-                        x_copy(s, u, g).wait_send()
-
-            return carry
-
-        lax.fori_loop(0, F, summed, 0)
+        late_left()
 
     vmem = pltpu.VMEM
     scratch = [

time: 134 us -> 130 us (0.970)
  Pallas kernels: 132 us -> 128 us
    pallas_call x1, Pallas kernels: 132 us -> 128 us  [local(): call(activations, *small, out_weight, up_weight, down_weight, norm_gain.r...]
where the time goes in v3:
time: 130 us
  Pallas kernels  128 us (98%)
  local copies, waits for them, and re-layouts  1.77 us (1%)
    pallas_call x1, Pallas kernels, local(): call(activations, *small, out_weight, up_weight, down_weight, norm_gain.r...  128 us

profile of v3, /device:TPU:12, one launch (start us, length us, event | category | flops | bytes accessed | tf_op | source)
XLA Modules:
  0.0 130.0 jit_solution(4942817436523241480)
XLA Ops:
  0.0 128.2 %layer.1 = bf16[384,512]{1,0:T(8,128)(2,1)} custom-call(bf16[384,512]{1,0:T(8,128)(2,1)} %refs_0_.1, bf16[512,128]{1,0:T(8,128)(2,1)} %refs_1_.1, bf16[512,128]{1,0:T(8,128)(2,1)} %refs_2_.1, bf16[512,128]{1,0:T(8,128)(2,1)} %refs_3_.1, bf16[512,128]{1,0:T(8,128)(2,1)} %refs_4_.1, bf16[128,512]{1,0:T(8,128)(2,1)} %refs_5_.1, bf16[512,2048]{1,0:T(8,128)(2,1)} %refs_6_.1, ...), custom_call_target="tpu_custom_call" | custom-call | tf_op jit(solution)/shard_map/layer/pallas_call | solution.py:926
  128.2 1.8 %copy.15 = bf16[384,512]{1,0:T(8,128)(2,1)} copy(bf16[384,512]{1,0:T(8,128)(2,1)} %layer.1) | data formatting | bytes 786432

commit v4 on v3

--- a/solution.py
+++ b/solution.py
@@ -159,10 +159,10 @@
         ("pd", 3, 0),
     ),
     ("low", 2, 0): (
+        ("pd", 3, 2),
+    ),
+    ("set", 0, 1): (
         ("pd", 3, 1),
-    ),
-    ("set", 0, 1): (
-        ("pd", 3, 2),
     ),
     ("low", 2, 1): (
         ("pd", 3, 3),

time: 130 us -> 129 us (level)
  no operation moved by 1% of the time
where the time goes in v4:
time: 129 us
  Pallas kernels  127 us (98%)
  local copies, waits for them, and re-layouts  1.77 us (1%)
    pallas_call x1, Pallas kernels, local(): call(activations, *small, out_weight, up_weight, down_weight, norm_gain.r...  127 us

profile of v4, /device:TPU:12, one launch (start us, length us, event | category | flops | bytes accessed | tf_op | source)
XLA Modules:
  0.0 129.0 jit_solution(7087207648115195987)
XLA Ops:
  0.0 127.3 %layer.1 = bf16[384,512]{1,0:T(8,128)(2,1)} custom-call(bf16[384,512]{1,0:T(8,128)(2,1)} %refs_0_.1, bf16[512,128]{1,0:T(8,128)(2,1)} %refs_1_.1, bf16[512,128]{1,0:T(8,128)(2,1)} %refs_2_.1, bf16[512,128]{1,0:T(8,128)(2,1)} %refs_3_.1, bf16[512,128]{1,0:T(8,128)(2,1)} %refs_4_.1, bf16[128,512]{1,0:T(8,128)(2,1)} %refs_5_.1, bf16[512,2048]{1,0:T(8,128)(2,1)} %refs_6_.1, ...), custom_call_target="tpu_custom_call" | custom-call | tf_op jit(solution)/shard_map/layer/pallas_call | solution.py:926
  127.3 1.8 %copy.15 = bf16[384,512]{1,0:T(8,128)(2,1)} copy(bf16[384,512]{1,0:T(8,128)(2,1)} %layer.1) | data formatting | bytes 786432
